TPU v7x, 32 devices: a whole 2x2x4 slice. The times are simulated.
32 devices in a mesh: ep: 8 (over z, core), tp: 4 (over y, x).
Axes of the slice: x: 2, y: 2, z: 4, core: 2. Of those that a mesh axis runs over, the one named last changes fastest.
Arguments:
- pool_input: bfloat16 [2048, 2048], P('ep'), may hold values from -6 to 6
- pool_gain: float32 [2048], replicated, may hold values from 0.1 to 1.9
- pool_weight: bfloat16 [512, 2048], P(None, 'tp'), may hold values from -0.25 to 0.25
- pool_scale: float32 [2048], P('tp'), may hold values from 0.1 to 1.9
- moe_input: bfloat16 [1536, 2048], P('ep'), may hold values from -6 to 6
- moe_gain: float32 [2048], replicated, may hold values from 0.1 to 1.9
- routes: int32 [1536, 2], P('ep'), may hold values from 0 to 7, all different within a row; in each aligned block of 192 rows (0 to 191, 192 to 383, ...) at most 96 rows name the same one
- route_logits: float32 [1536, 2], P('ep'), may hold values from -4 to 4
- gate_weight: bfloat16 [8, 2048, 4096], P('ep', None, 'tp'), may hold values from -0.125 to 0.125
- up_weight: bfloat16 [8, 2048, 4096], P('ep', None, 'tp'), may hold values from -0.125 to 0.125
- down_weight: bfloat16 [8, 2048, 4096], P('ep', None, 'tp'), may hold values from -0.09375 to 0.09375
Outputs:
- pool_out: bfloat16 [2048, 2048], P('ep', 'tp')
- expert_out: bfloat16 [1536, 2048], P('ep', 'tp')
Inputs may be any that keep to these rules, and one draw needn't show every extreme that they name: `routes`: the 2 experts of a token differ. Within the rows of one device (aligned blocks of 192 rows) no expert is named by more than 96 rows, and in every draw some expert is named by exactly 96 rows of some device.
All inputs are finite; a program needn't handle non-finite values.
Results may differ from a plain program's by a relative error of at most 0.017.
Values may be sent and summed in bfloat16 or wider, within the bound.
A program may use at most 64 MiB of HBM per device.

v0:
```python
import jax
import jax.numpy as jnp
from jax import lax
from jax.sharding import PartitionSpec as P

GROUP_WIDTH = 512
EPSILON = 1e-06
halo_rows = 15


def passed_along(value, axis, steps):
    count = lax.axis_size(axis)
    leading, last = (max(0, -steps), min(count, count - steps))
    return lax.ppermute(value, axis, [(source, source + steps) for source in range(leading, last)])


def rms_rows(row_block, scale_gain):
    values = row_block.astype(jnp.float32)
    scaled = values * lax.rsqrt(jnp.mean(values * values, axis=-1, keepdims=True) + EPSILON)
    return (scaled * scale_gain).astype(jnp.bfloat16)


def delayed(values, offset):
    return jnp.concatenate(
        [jnp.zeros((offset,) + values.shape[1:], values.dtype), values[:-offset]], axis=0
    )


def window_sums(values):
    totals = []
    current = values
    for offset in (1, 2, 4, 8):
        current = current + delayed(current, offset)
        totals.append(current)
    return totals


def slot_tables(route_block, expert_count, capacity):
    tokens_count = route_block.shape[0]
    picks_count = route_block.shape[1]
    flat_ids = route_block.reshape(-1)
    onehot = (flat_ids[:, None] == jnp.arange(expert_count, dtype=jnp.int32)[None, :]).astype(
        jnp.int32
    )
    before = jnp.cumsum(onehot, axis=0) - onehot
    rank_in = jnp.sum(before * onehot, axis=1)
    slot_ids = flat_ids * capacity + rank_in
    owners = jnp.repeat(jnp.arange(tokens_count, dtype=jnp.int32), picks_count)
    holder = jnp.full((expert_count * capacity,), tokens_count, jnp.int32).at[slot_ids].set(owners)
    return (slot_ids, holder)


def pool_half(pool_input, pool_gain, pool_weight, pool_scale):
    normed = rms_rows(pool_input, pool_gain)
    local_rows = normed.shape[0]
    column_count = pool_weight.shape[1]
    group_index = lax.axis_index("tp") * column_count // GROUP_WIDTH
    own_group = lax.dynamic_slice_in_dim(normed, group_index * GROUP_WIDTH, GROUP_WIDTH, 1)
    earlier = passed_along(own_group[local_rows - halo_rows :], "ep", 1)
    extended = jnp.concatenate([earlier, own_group], axis=0).astype(jnp.float32)
    stacked = jnp.stack(window_sums(extended))[:, halo_rows:]
    chosen = lax.dynamic_index_in_dim(stacked, group_index, 0, keepdims=False)
    position = lax.axis_index("ep") * local_rows + lax.iota(jnp.int32, local_rows)
    window = jnp.left_shift(jnp.int32(2), group_index)
    counts = jnp.minimum(position + 1, window).astype(jnp.float32)
    mixed_in = (chosen / counts[:, None] - own_group.astype(jnp.float32)).astype(jnp.bfloat16)
    product = jnp.dot(mixed_in, pool_weight, preferred_element_type=jnp.float32)
    return (product * pool_scale).astype(jnp.bfloat16)


def expert_half(moe_input, moe_gain, routes, route_logits, gate_weight, up_weight, down_weight):
    normed = rms_rows(moe_input, moe_gain)
    local_rows, row_width = normed.shape
    picks_count = routes.shape[1]
    experts = lax.axis_size("ep")
    capacity = 2 * local_rows * picks_count // experts
    slot_ids, holder = slot_tables(routes, experts, capacity)
    padded = jnp.concatenate([normed, jnp.zeros((1, row_width), jnp.bfloat16)], axis=0)
    gate_block = gate_weight[0]
    up_block = up_weight[0]
    down_block = down_weight[0]
    column_count = row_width // lax.axis_size("tp")
    start_col = lax.axis_index("tp") * column_count
    narrow = lax.dynamic_slice_in_dim(padded, start_col, column_count, 1)
    outgoing = narrow[holder].reshape(experts, capacity, column_count)
    arrived = lax.all_to_all(outgoing, "ep", split_axis=0, concat_axis=0, tiled=True).reshape(
        experts * capacity, column_count
    )
    segment = lax.all_gather(arrived, "tp", axis=1, tiled=True)
    gate_part = jnp.dot(segment, gate_block, preferred_element_type=jnp.float32)
    up_part = jnp.dot(segment, up_block, preferred_element_type=jnp.float32)
    hidden = (jax.nn.silu(gate_part) * up_part).astype(jnp.bfloat16)
    summed = lax.psum_scatter(
        lax.dot_general(
            down_block, hidden, (((1,), (1,)), ((), ())), preferred_element_type=jnp.float32
        ).astype(jnp.bfloat16),
        "tp",
        scatter_dimension=0,
        tiled=True,
    ).astype(jnp.float32)
    results = summed.astype(jnp.bfloat16).reshape(summed.shape[0], experts, capacity)
    returned = lax.all_to_all(results, "ep", split_axis=1, concat_axis=1, tiled=True).reshape(
        summed.shape[0], experts * capacity
    )
    picked = (
        returned[:, slot_ids].astype(jnp.float32).reshape(summed.shape[0], local_rows, picks_count)
    )
    raised = jnp.exp(route_logits)
    shares = raised / jnp.sum(raised, axis=-1, keepdims=True)
    combined = jnp.einsum("dtk,tk->td", picked, shares)
    return combined.astype(jnp.bfloat16)


def local(
    pool_input,
    pool_gain,
    pool_weight,
    pool_scale,
    moe_input,
    moe_gain,
    routes,
    route_logits,
    gate_weight,
    up_weight,
    down_weight,
):
    pool_out = pool_half(pool_input, pool_gain, pool_weight, pool_scale)
    expert_out = expert_half(
        moe_input, moe_gain, routes, route_logits, gate_weight, up_weight, down_weight
    )
    return (pool_out, expert_out)


def solution(mesh):
    in_specs = (
        P("ep", None),
        P(),
        P(None, "tp"),
        P("tp"),
        P("ep", None),
        P(),
        P("ep", None),
        P("ep", None),
        P("ep", None, "tp"),
        P("ep", None, "tp"),
        P("ep", None, "tp"),
    )
    out_specs = (P("ep", "tp"), P("ep", "tp"))
    return jax.shard_map(local, mesh=mesh, in_specs=in_specs, out_specs=out_specs, check_vma=False)
```

profile of v0, /device:TPU:0, one launch (start us, length us, event | category | flops | bytes accessed | tf_op | source)
XLA Modules:
  0.0 184.2 jit_solution(8326187543108541298)
XLA Ops:
  7.2 0.8 copy.14
  8.1 0.1 eq.29
  8.2 0.1 eq.25
  8.4 0.7 broadcast_multiply_fusion
  9.1 1.4 fusion.14
  10.4 0.9 reduce-window.6
  11.3 0.2 slice_reduce_fusion
  11.7 0.1 mul.99
  12.1 2.9 %scatter_custom_fusion = s32[768]{0:T(1024)S(1)} fusion(s32[384]{0:T(512)S(1)} %fusion.33, s32[384]{0:T(512)S(1)} %reshape.122, s32[]{:T(128)} %constant.67.clone.1), kind=kCustom, calls=%fused_computation.53 | custom fusion | bytes 3076 | tf_op jit(solution)/shard_map/scatter | solution.py:49
  15.1 1.4 fusion.16
  16.5 2.7 %gather_fusion = bf16[768,512]{1,0:T(8,128)(2,1)S(1)} fusion(bf16[193,512]{1,0:T(8,128)(2,1)S(1)} %pad_dynamic-slice_fusion.4, s32[1024]{0:T(1024)S(1)} %pad_clamp_fusion.1), kind=kCustom, calls=%fused_computation | custom fusion | bytes 1575936 | tf_op jit(solution)/shard_map/gather | solution.py:85
  19.2 27.2 %all_to_all.10 = bf16[8,96,512]{2,1,0:T(8,128)(2,1)} all-to-all(bf16[8,96,512]{2,1,0:T(8,128)(2,1)S(1)} %bitcast.67), channel_id=1, replica_groups=mesh['ep'=8,'tp'=4] {'ep'}, dimensions={0} | all-to-all | bytes 1572864 | tf_op jit(solution)/shard_map/all_to_all | solution.py:86
  46.5 42.8 %all-gather.2.cloned.1.call-done = bf16[768,2048]{1,0:T(8,128)(2,1)} async-done(((bf16[768,512]{1,0:T(8,128)(2,1)}), bf16[768,2048]{1,0:T(8,128)(2,1)}) %all-gather.2.cloned.1.call-update) | async-done | bytes 3145744 | tf_op jit(solution)/shard_map/all_gather | solution.py:89
  89.2 6.3 %fusion.2 = f32[768,1024]{1,0:T(8,128)S(1)} fusion(bf16[768,2048]{1,0:T(8,128)(2,1)} %all-gather.2.cloned.1.call-done, bf16[1,2048,1024]{2,1,0:T(8,128)(2,1)} %param.20), kind=kOutput, calls=%fused_computation.5 | convolution fusion | flops 3221225472 | bytes 10485760 | tf_op jit(solution)/shard_map/dot_general | solution.py:91
  95.5 3.8 %multiply_convert_fusion = bf16[768,1024]{1,0:T(8,128)(2,1)S(1)} fusion(f32[768,1024]{1,0:T(8,128)S(1)} %fusion.2, bf16[768,2048]{1,0:T(8,128)(2,1)S(1)} %copy-done.5, bf16[1,2048,1024]{2,1,0:T(8,128)(2,1)S(1)} %copy-done.3), kind=kOutput, calls=%fused_computation.10 | convolution fusion | flops 3225944064 | bytes 12058624 | tf_op jit(solution)/shard_map/dot_general | solution.py:90
  99.4 4.9 %fusion.9 = bf16[2048,768]{0,1:T(8,128)(2,1)} fusion(bf16[768,1024]{1,0:T(8,128)(2,1)S(1)} %multiply_convert_fusion, bf16[1,2048,1024]{2,1,0:T(8,128)(2,1)S(1)} %copy-done.4), kind=kOutput, calls=%fused_computation.11 | convolution fusion | flops 3222798336 | bytes 8912896 | tf_op jit(solution)/shard_map/dot_general | solution.py:94
  104.3 1.2 copy-done.1
  105.5 1.6 convert_element_type.53
  107.1 0.8 dynamic-slice
  107.9 0.3 multiply_reduce_fusion
  108.1 1.2 fusion.25
  109.3 1.6 collective-permute-start
  111.0 37.4 %reduce-scatter.2.cloned.1.call-done = bf16[512,768]{0,1:T(8,128)(2,1)} async-done(((bf16[2048,768]{0,1:T(8,128)(2,1)}), bf16[512,768]{0,1:T(8,128)(2,1)}) %reduce-scatter.2.cloned.1.call-update) | async-done | bytes 786448 | tf_op jit(solution)/shard_map/reduce_scatter | solution.py:93
  148.3 4.6 %all-to-all-start.1 = ((bf16[512,8,96]{0,2,1:T(8,128)(2,1)}), bf16[512,8,96]{0,2,1:T(8,128)(2,1)S(1)}, u32[]{:S(2)}, u32[]{:S(2)}) async-start(bf16[512,8,96]{0,2,1:T(8,128)(2,1)} %bitcast.71), calls=%async_computation.2 | async-start | bytes 1572864 | tf_op jit(solution)/shard_map/all_to_all | solution.py:102
  153.0 0.2 copy.16
  153.8 0.3 copy-done.6
  154.1 1.2 fusion.17
  155.3 18.6 %all-to-all-done.1 = bf16[512,8,96]{0,2,1:T(8,128)(2,1)S(1)} async-done(((bf16[512,8,96]{0,2,1:T(8,128)(2,1)}), bf16[512,8,96]{0,2,1:T(8,128)(2,1)S(1)}, u32[]{:S(2)}, u32[]{:S(2)}) %all-to-all-start.1) | async-done | bytes 786464 | tf_op jit(solution)/shard_map/all_to_all | solution.py:102
  173.9 2.1 %gather_fusion.1 = bf16[384,512]{1,0:T(8,128)(2,1)S(1)} fusion(bf16[512,768]{0,1:T(8,128)(2,1)S(1)} %bitcast.61, s32[1024]{0:T(1024)S(1)} %pad_clamp_fusion), kind=kCustom, calls=%fused_computation.1 | custom fusion | bytes 787968 | tf_op jit(solution)/shard_map/gather | solution.py:106
  176.0 0.2 reshape.101
  176.1 0.6 fusion.36
  176.7 0.7 copy.19
  (40 shorter events, 1.2 us)
Async XLA Ops:
  7.2 146.6 %copy-start = (bf16[512,512]{1,0:T(8,128)(2,1)S(1)}, bf16[512,512]{1,0:T(8,128)(2,1)}, u32[]{:S(2)}) copy-start(bf16[512,512]{1,0:T(8,128)(2,1)} %param.13) | copy-start | bytes 1572868
  7.2 82.0 %all-gather.2.cloned.1.call-start = ((), (), s32[]{:S(2)}) async-start(), calls=%async_computation.3 | async-start | bytes 3932160 | tf_op jit(solution)/shard_map/all_gather | solution.py:89
  46.4 101.9 %reduce-scatter.2.cloned.1.call-start = ((), (), s32[]{:S(2)}) async-start(), calls=%async_computation.4 | async-start | bytes 3932160 | tf_op jit(solution)/shard_map/reduce_scatter | solution.py:93
  89.2 6.3 %copy-start.3 = (bf16[1,2048,1024]{2,1,0:T(8,128)(2,1)S(1)}, bf16[1,2048,1024]{2,1,0:T(8,128)(2,1)}, u32[]{:S(2)}) copy-start(bf16[1,2048,1024]{2,1,0:T(8,128)(2,1)} %param.19) | copy-start | bytes 12582916
  89.2 6.3 %copy-start.5 = (bf16[768,2048]{1,0:T(8,128)(2,1)S(1)}, bf16[768,2048]{1,0:T(8,128)(2,1)}, u32[]{:S(2)}) copy-start(bf16[768,2048]{1,0:T(8,128)(2,1)} %all-gather.2.cloned.1.call-done) | copy-start | bytes 9437188
  95.5 3.8 %copy-start.4 = (bf16[1,2048,1024]{2,1,0:T(8,128)(2,1)S(1)}, bf16[1,2048,1024]{2,1,0:T(8,128)(2,1)}, u32[]{:S(2)}) copy-start(bf16[1,2048,1024]{2,1,0:T(8,128)(2,1)} %param.21) | copy-start | bytes 12582916
  104.3 1.2 copy-start.1
  104.3 6.6 %copy-start.2 = (f32[192,2]{0,1:T(2,128)S(1)}, f32[192,2]{0,1:T(2,128)}, u32[]{:S(2)}) copy-start(f32[192,2]{0,1:T(2,128)} %param.18) | copy-start | bytes 4612
  109.3 43.8 %collective-permute-start = (bf16[15,512]{1,0:T(8,128)(2,1)S(1)}, bf16[15,512]{1,0:T(8,128)(2,1)S(1)}, u32[]{:S(2)}, u32[]{:S(2)}) collective-permute-start(bf16[15,512]{1,0:T(8,128)(2,1)S(1)} %slice.36), channel_id=1, source_target_pairs={{0,4},{4,8},{8,12},{12,16},{16,20},{20,24},{24,28},{1,5},{5,9},{9,... | collective-permute-start | bytes 46088 | tf_op jit(solution)/shard_map/ppermute | solution.py:14
  148.3 25.6 %all-to-all-start.1 = ((bf16[512,8,96]{0,2,1:T(8,128)(2,1)}), bf16[512,8,96]{0,2,1:T(8,128)(2,1)S(1)}, u32[]{:S(2)}, u32[]{:S(2)}) async-start(bf16[512,8,96]{0,2,1:T(8,128)(2,1)} %bitcast.71), calls=%async_computation.2 | async-start | bytes 1572864 | tf_op jit(solution)/shard_map/all_to_all | solution.py:102
  153.4 0.7 copy-start.6
Sparse Core Ops, SparseCore 0:
  46.5 42.6 all-gather.1
  104.4 43.8 reduce-scatter.1
where the time goes:
time: 185 us; the launch traced here: 184 us
  waiting for transfers between devices  98.8 us (53%)
  blocking collectives  27.2 us (15%)
  matrix products  16.7 us (9%)
  between operations  14.4 us (8%)
  local copies, waits for them, and re-layouts  12.8 us (7%)
  other arithmetic  8.08 us (4%)
  starting transfers between devices  6.26 us (3%)
    all_gather x1, waiting for transfers between devices, expert_half(): segment = lax.all_gather(arrived, 'tp', axis=1, tiled=True)  42.8 us
    reduce_scatter x1, waiting for transfers between devices, expert_half(): lax.psum_scatter(lax.dot_general(down_block, hidden, (((1,), (1,)), ((),...  37.4 us
    all_to_all x1, blocking collectives, expert_half(): lax.all_to_all(outgoing, 'ep', split_axis=0, concat_axis=0, tiled=True)  27.2 us
    all_to_all x1, waiting for transfers between devices, expert_half(): lax.all_to_all(results, 'ep', split_axis=1, concat_axis=1, tiled=True)  18.6 us
    dot_general x1, matrix products, expert_half(): up_part = jnp.dot(segment, up_block, preferred_element_type=jnp.float32)  6.28 us
    dot_general x1, matrix products, expert_half(): lax.dot_general(down_block, hidden, (((1,), (1,)), ((), ())), preferred_e...  4.88 us
    all_to_all x1, starting transfers between devices, expert_half(): lax.all_to_all(results, 'ep', split_axis=1, concat_axis=1, tiled=True)  4.61 us
    dot_general x1, matrix products, expert_half(): gate_part = jnp.dot(segment, gate_block, preferred_element_type=jnp.float32)  3.82 us
  transfers between devices with their start and end apart: 4, of which 3 were waited for; matrix products, arithmetic and copies ran while one was open for 3% of the time, Pallas kernels for 0%

commit v1 on v0

--- a/solution.py
+++ b/solution.py
@@ -86,7 +86,16 @@
     arrived = lax.all_to_all(outgoing, "ep", split_axis=0, concat_axis=0, tiled=True).reshape(
         experts * capacity, column_count
     )
-    segment = lax.all_gather(arrived, "tp", axis=1, tiled=True)
+    lanes = lax.axis_size("tp")
+    arr_next = arrived
+    all_blocks = [arr_next]
+    small = sorted(((k, (k + 1) % lanes) for k in range(lanes)))
+    for pp in range(1, lanes):
+        arr_next = lax.ppermute(arr_next, axis_name="tp", perm=small)
+        all_blocks.insert(0, arr_next)
+    e_now = jnp.concatenate(all_blocks, axis=1)
+    x_new = lax.axis_index("tp") + 1
+    segment = jnp.roll(e_now, x_new * arrived.shape[1], axis=1)
     gate_part = jnp.dot(segment, gate_block, preferred_element_type=jnp.float32)
     up_part = jnp.dot(segment, up_block, preferred_element_type=jnp.float32)
     hidden = (jax.nn.silu(gate_part) * up_part).astype(jnp.bfloat16)

time: 185 us -> 199 us (1.076)
  waiting for transfers between devices: 98.8 us -> 112 us
  matrix products: 16.7 us -> 13.8 us
  local copies, waits for them, and re-layouts: 12.8 us -> 15.1 us
    ppermute x0 -> x3, waiting for transfers between devices: none -> 54.9 us  [expert_half(): arr_next = lax.ppermute(arr_next, axis_name='tp', perm=small)]
    all_gather x1 -> x0, waiting for transfers between devices: 42.8 us -> none  [expert_half(): segment = lax.all_gather(arrived, 'tp', axis=1, tiled=True)]
    dot_general x1, matrix products: 6.28 us -> 3.76 us  [expert_half(): up_part = jnp.dot(segment, up_block, preferred_element_type=jnp.float32)]
    unnamed x15 -> x22, local copies, waits for them, and re-layouts: 2.34 us -> 4.57 us
    ppermute x0 -> x3, starting transfers between devices: none -> 2.09 us  [expert_half(): arr_next = lax.ppermute(arr_next, axis_name='tp', perm=small)]
  transfers between devices with their start and end apart: 4 -> 6, of which waited for: 3 -> 5; matrix products, arithmetic and copies ran while one was open for 3% -> 3% of each run, Pallas kernels for 0% -> 0%
where the time goes in v1:
time: 199 us
  waiting for transfers between devices  112 us (56%)
  blocking collectives  27.1 us (14%)
  local copies, waits for them, and re-layouts  15.1 us (8%)
  between operations  14.4 us (7%)
  matrix products  13.8 us (7%)
  other arithmetic  8.09 us (4%)
  starting transfers between devices  8.04 us (4%)
    ppermute x3, waiting for transfers between devices, expert_half(): arr_next = lax.ppermute(arr_next, axis_name='tp', perm=small)  54.9 us
    reduce_scatter x1, waiting for transfers between devices, expert_half(): lax.psum_scatter(lax.dot_general(down_block, hidden, (((1,), (1,)), ((),...  38.6 us
    all_to_all x1, blocking collectives, expert_half(): lax.all_to_all(outgoing, 'ep', split_axis=0, concat_axis=0, tiled=True)  27.1 us
    all_to_all x1, waiting for transfers between devices, expert_half(): lax.all_to_all(results, 'ep', split_axis=1, concat_axis=1, tiled=True)  18.9 us
    dot_general x1, matrix products, expert_half(): lax.dot_general(down_block, hidden, (((1,), (1,)), ((), ())), preferred_e...  4.89 us
    all_to_all x1, starting transfers between devices, expert_half(): lax.all_to_all(results, 'ep', split_axis=1, concat_axis=1, tiled=True)  4.62 us
    unnamed x22, local copies, waits for them, and re-layouts  4.57 us
  transfers between devices with their start and end apart: 6, of which 5 were waited for; matrix products, arithmetic and copies ran while one was open for 3% of the time, Pallas kernels for 0%

profile of v1, /device:TPU:0, one launch (start us, length us, event | category | flops | bytes accessed | tf_op | source)
XLA Modules:
  0.0 199.0 jit_solution(13807569217259432192)
XLA Ops:
  7.2 0.8 copy.14
  8.4 0.7 broadcast_multiply_fusion
  9.1 1.4 fusion.18
  10.4 0.9 reduce-window.6
  11.3 0.2 slice_reduce_fusion
  12.1 2.9 %scatter_custom_fusion = s32[768]{0:T(1024)S(1)} fusion(s32[384]{0:T(512)S(1)} %fusion.40, s32[384]{0:T(512)S(1)} %reshape.122, s32[]{:T(128)} %constant.86.clone.1), kind=kCustom, calls=%fused_computation.63 | custom fusion | bytes 3076 | tf_op jit(solution)/shard_map/scatter | solution.py:49
  15.1 1.4 fusion.20
  16.5 2.7 %gather_fusion = bf16[768,512]{1,0:T(8,128)(2,1)S(1)} fusion(bf16[193,512]{1,0:T(8,128)(2,1)S(1)} %pad_dynamic-slice_fusion.4, s32[1024]{0:T(1024)S(1)} %pad_clamp_fusion.1), kind=kCustom, calls=%fused_computation | custom fusion | bytes 1575936 | tf_op jit(solution)/shard_map/gather | solution.py:85
  19.2 27.1 %all_to_all.10 = bf16[8,96,512]{2,1,0:T(8,128)(2,1)S(1)} all-to-all(bf16[8,96,512]{2,1,0:T(8,128)(2,1)S(1)} %bitcast.68), channel_id=1, replica_groups=mesh['ep'=8,'tp'=4] {'ep'}, dimensions={0} | all-to-all | bytes 1572864 | tf_op jit(solution)/shard_map/all_to_all | solution.py:86
  46.3 1.5 collective-permute-start.1
  47.8 18.3 %collective-permute-done.1 = bf16[768,512]{1,0:T(8,128)(2,1)S(1)} collective-permute-done((bf16[768,512]{1,0:T(8,128)(2,1)S(1)}, bf16[768,512]{1,0:T(8,128)(2,1)S(1)}, u32[]{:S(2)}, u32[]{:S(2)}) %collective-permute-start.1) | collective-permute-done | bytes 786464 | tf_op jit(solution)/shard_map/ppermute | solution.py:94
  66.1 0.6 collective-permute-start.2
  66.7 18.4 %collective-permute-done.2 = bf16[768,512]{1,0:T(8,128)(2,1)S(1)} collective-permute-done((bf16[768,512]{1,0:T(8,128)(2,1)S(1)}, bf16[768,512]{1,0:T(8,128)(2,1)S(1)}, u32[]{:S(2)}, u32[]{:S(2)}) %collective-permute-start.2) | collective-permute-done | bytes 786464 | tf_op jit(solution)/shard_map/ppermute | solution.py:94
  85.1 18.2 %collective-permute-done.3 = bf16[768,512]{1,0:T(8,128)(2,1)} collective-permute-done((bf16[768,512]{1,0:T(8,128)(2,1)S(1)}, bf16[768,512]{1,0:T(8,128)(2,1)}, u32[]{:S(2)}, u32[]{:S(2)}) %collective-permute-start.3) | collective-permute-done | bytes 786464 | tf_op jit(solution)/shard_map/ppermute | solution.py:94
  103.3 1.2 constant_dynamic-update-slice_fusion.7
  104.8 1.4 constant_dynamic-update-slice_fusion.3
  106.5 0.6 copy-done.3
  107.1 3.4 %fusion.4 = f32[768,1024]{1,0:T(8,128)S(1)} fusion(bf16[1,2048,1024]{2,1,0:T(8,128)(2,1)S(1)} %copy-done.3, bf16[768,4096]{1,0:T(8,128)(2,1)S(1)} %constant_dynamic-update-slice_fusion, s32[]{:T(128)S(6)} %select_n.48), kind=kOutput, calls=%fused_computation.7 | convolution fusion | flops 3221225472 | bytes 10485764 | tf_op jit(solution)/shard_map/dot_general | solution.py:99
  110.6 3.8 %multiply_convert_fusion = bf16[768,1024]{1,0:T(8,128)(2,1)S(1)} fusion(f32[768,1024]{1,0:T(8,128)S(1)} %fusion.4, bf16[1,2048,1024]{2,1,0:T(8,128)(2,1)S(1)} %copy-done.4, bf16[768,4096]{1,0:T(8,128)(2,1)S(1)} %constant_dynamic-update-slice_fusion, s32[]{:T(128)S(6)} %select_n.48), kind=kOutput, calls=%fused_computation.10 | convolution fusion | flops 3225944064 | bytes 12058628 | tf_op jit(solution)/shard_map/dot_general | solution.py:100
  114.4 4.9 %fusion.9 = bf16[2048,768]{0,1:T(8,128)(2,1)} fusion(bf16[768,1024]{1,0:T(8,128)(2,1)S(1)} %multiply_convert_fusion, bf16[1,2048,1024]{2,1,0:T(8,128)(2,1)S(1)} %copy-done.5), kind=kOutput, calls=%fused_computation.11 | convolution fusion | flops 3222798336 | bytes 8912896 | tf_op jit(solution)/shard_map/dot_general | solution.py:103
  119.3 1.6 convert_element_type.53
  120.9 0.8 dynamic-slice
  121.7 0.3 multiply_reduce_fusion
  122.0 1.2 fusion.29
  123.1 1.3 collective-permute-start
  124.5 38.6 %reduce-scatter.2.cloned.1.call-done = bf16[512,768]{0,1:T(8,128)(2,1)} async-done(((bf16[2048,768]{0,1:T(8,128)(2,1)}), bf16[512,768]{0,1:T(8,128)(2,1)}) %reduce-scatter.2.cloned.1.call-update) | async-done | bytes 786448 | tf_op jit(solution)/shard_map/reduce_scatter | solution.py:102
  163.1 4.6 %all-to-all-start.1 = ((bf16[512,8,96]{0,2,1:T(8,128)(2,1)}), bf16[512,8,96]{0,2,1:T(8,128)(2,1)S(1)}, u32[]{:S(2)}, u32[]{:S(2)}) async-start(bf16[512,8,96]{0,2,1:T(8,128)(2,1)} %bitcast.71), calls=%async_computation.2 | async-start | bytes 1572864 | tf_op jit(solution)/shard_map/all_to_all | solution.py:111
  168.6 1.2 fusion.21
  169.8 18.9 %all-to-all-done.1 = bf16[512,8,96]{0,2,1:T(8,128)(2,1)S(1)} async-done(((bf16[512,8,96]{0,2,1:T(8,128)(2,1)}), bf16[512,8,96]{0,2,1:T(8,128)(2,1)S(1)}, u32[]{:S(2)}, u32[]{:S(2)}) %all-to-all-start.1) | async-done | bytes 786464 | tf_op jit(solution)/shard_map/all_to_all | solution.py:111
  188.7 2.1 %gather_fusion.1 = bf16[384,512]{1,0:T(8,128)(2,1)S(1)} fusion(bf16[512,768]{0,1:T(8,128)(2,1)S(1)} %bitcast.59, s32[1024]{0:T(1024)S(1)} %pad_clamp_fusion), kind=kCustom, calls=%fused_computation.1 | custom fusion | bytes 787968 | tf_op jit(solution)/shard_map/gather | solution.py:115
  190.9 0.6 fusion.42
  191.5 0.7 copy.19
  (51 shorter events, 2.4 us)
Async XLA Ops:
  7.2 161.4 %copy-start = (bf16[512,512]{1,0:T(8,128)(2,1)S(1)}, bf16[512,512]{1,0:T(8,128)(2,1)}, u32[]{:S(2)}) copy-start(bf16[512,512]{1,0:T(8,128)(2,1)} %param.13) | copy-start | bytes 1572868
  7.2 155.9 %reduce-scatter.2.cloned.1.call-start = ((), (), s32[]{:S(2)}) async-start(), calls=%async_computation.3 | async-start | bytes 3932160 | tf_op jit(solution)/shard_map/reduce_scatter | solution.py:102
  46.3 19.8 %collective-permute-start.1 = (bf16[768,512]{1,0:T(8,128)(2,1)S(1)}, bf16[768,512]{1,0:T(8,128)(2,1)S(1)}, u32[]{:S(2)}, u32[]{:S(2)}) collective-permute-start(bf16[768,512]{1,0:T(8,128)(2,1)S(1)} %bitcast.60), channel_id=1, source_target_pairs={{0,1},{1,2},{2,3},{3,0},{4,5},{5,6},{6,7},{7,4},{8,9},{9,10},{10,1... | collective-permute-start | bytes 2359304 | tf_op jit(solution)/shard_map/ppermute | solution.py:94
  66.1 19.0 %collective-permute-start.2 = (bf16[768,512]{1,0:T(8,128)(2,1)S(1)}, bf16[768,512]{1,0:T(8,128)(2,1)S(1)}, u32[]{:S(2)}, u32[]{:S(2)}) collective-permute-start(bf16[768,512]{1,0:T(8,128)(2,1)S(1)} %collective-permute-done.1), channel_id=1, source_target_pairs={{0,1},{1,2},{2,3},{3,0},{4,5},{5,6},{6,7},{7,4},{8,9},{9,10},{10,1... | collective-permute-start | bytes 2359304 | tf_op jit(solution)/shard_map/ppermute | solution.py:94
  85.0 18.2 %collective-permute-start.3 = (bf16[768,512]{1,0:T(8,128)(2,1)S(1)}, bf16[768,512]{1,0:T(8,128)(2,1)}, u32[]{:S(2)}, u32[]{:S(2)}) collective-permute-start(bf16[768,512]{1,0:T(8,128)(2,1)S(1)} %collective-permute-done.2), channel_id=1, source_target_pairs={{0,1},{1,2},{2,3},{3,0},{4,5},{5,6},{6,7},{7,4},{8,9},{9,10},{10,1... | collective-permute-start | bytes 2359304 | tf_op jit(solution)/shard_map/ppermute | solution.py:94
  104.7 2.4 %copy-start.3 = (bf16[1,2048,1024]{2,1,0:T(8,128)(2,1)S(1)}, bf16[1,2048,1024]{2,1,0:T(8,128)(2,1)}, u32[]{:S(2)}) copy-start(bf16[1,2048,1024]{2,1,0:T(8,128)(2,1)} %param.19) | copy-start | bytes 12582916
  107.1 3.4 %copy-start.4 = (bf16[1,2048,1024]{2,1,0:T(8,128)(2,1)S(1)}, bf16[1,2048,1024]{2,1,0:T(8,128)(2,1)}, u32[]{:S(2)}) copy-start(bf16[1,2048,1024]{2,1,0:T(8,128)(2,1)} %param.20) | copy-start | bytes 12582916
  110.5 3.8 %copy-start.5 = (bf16[1,2048,1024]{2,1,0:T(8,128)(2,1)S(1)}, bf16[1,2048,1024]{2,1,0:T(8,128)(2,1)}, u32[]{:S(2)}) copy-start(bf16[1,2048,1024]{2,1,0:T(8,128)(2,1)} %param.21) | copy-start | bytes 12582916
  114.3 4.9 %copy-start.1 = (bf16[256,2048]{1,0:T(8,128)(2,1)S(1)}, bf16[256,2048]{1,0:T(8,128)(2,1)}, u32[]{:S(2)}) copy-start(bf16[256,2048]{1,0:T(8,128)(2,1)} %param.11) | copy-start | bytes 3145732
  119.2 5.2 %copy-start.2 = (f32[192,2]{0,1:T(2,128)S(1)}, f32[192,2]{0,1:T(2,128)}, u32[]{:S(2)}) copy-start(f32[192,2]{0,1:T(2,128)} %param.18) | copy-start | bytes 4612
  123.1 44.8 %collective-permute-start = (bf16[15,512]{1,0:T(8,128)(2,1)S(1)}, bf16[15,512]{1,0:T(8,128)(2,1)S(1)}, u32[]{:S(2)}, u32[]{:S(2)}) collective-permute-start(bf16[15,512]{1,0:T(8,128)(2,1)S(1)} %slice.36), channel_id=1, source_target_pairs={{0,4},{4,8},{8,12},{12,16},{16,20},{20,24},{24,28},{1,5},{5,9},{9,... | collective-permute-start | bytes 46088 | tf_op jit(solution)/shard_map/ppermute | solution.py:14
  163.1 25.6 %all-to-all-start.1 = ((bf16[512,8,96]{0,2,1:T(8,128)(2,1)}), bf16[512,8,96]{0,2,1:T(8,128)(2,1)S(1)}, u32[]{:S(2)}, u32[]{:S(2)}) async-start(bf16[512,8,96]{0,2,1:T(8,128)(2,1)} %bitcast.71), calls=%async_computation.2 | async-start | bytes 1572864 | tf_op jit(solution)/shard_map/all_to_all | solution.py:111
  167.8 0.8 copy-start.6
Sparse Core Ops, SparseCore 0:
  119.4 43.6 reduce-scatter.1
